TPU v7x, 32 devices: a whole 2x2x4 slice. The times are simulated.
32 devices in a mesh: sp: 4 (over z), fs: 4 (over y, x), tp: 2 (over core).
Axes of the slice: x: 2, y: 2, z: 4, core: 2. Of those that a mesh axis runs over, the one named last changes fastest.
Arguments:
- queries: bfloat16 [4, 1024, 512], P('fs', 'sp', 'tp'), may hold values from -60 to 60
- keys: bfloat16 [4, 1024, 256], P('fs', 'sp', 'tp'), may hold values from -4.5 to 4.5
- values: bfloat16 [4, 1024, 256], P('fs', 'sp', 'tp'), may hold values from -6 to 6
- forget_cache: float32 [4, 1024, 8], P('fs', 'sp', 'tp'), may hold values from -128 to 0, as said below
- fox_gain: float32 [512], P('tp'), may hold values from 0.1 to 1.9
- receptance: bfloat16 [4, 1024, 512], P('fs', 'sp', 'tp'), may hold values from -6 to 6
- lin_keys: bfloat16 [4, 1024, 512], P('fs', 'sp', 'tp'), may hold values from -6 to 6
- lin_values: bfloat16 [4, 1024, 512], P('fs', 'sp', 'tp'), may hold values from -6 to 6
- learn_logit: bfloat16 [4, 1024, 512], P('fs', 'sp', 'tp'), may hold values from -12 to 4
- decay_log: float32 [4, 1024, 512], P('fs', 'sp', 'tp'), may hold values from -16 to 0
- lin_gain: float32 [512], P('tp'), may hold values from 0.1 to 1.9
- out_fox_weight: bfloat16 [512, 2048], P('tp', 'fs'), may hold values from -0.1875 to 0.1875
- out_lin_weight: bfloat16 [512, 2048], P('tp', 'fs'), may hold values from -0.1875 to 0.1875
Outputs:
- mixed: bfloat16 [4, 1024, 2048], P('fs', ('sp', 'tp'))
Inputs may be any that keep to these rules, and one draw needn't show every extreme that they name: `forget_cache`: Non-increasing along the positions of each sequence and head.
All inputs are finite; a program needn't handle non-finite values.
Results may differ from a plain program's by a relative error of at most 0.017.
Values may be sent and summed in bfloat16 or wider, within the bound.
A program may use at most 64 MiB of HBM per device.

v0:
```python
import math

import jax
import jax.numpy as jnp
from jax import lax
from jax.sharding import PartitionSpec as P

HEAD = 64
SPAN = 64


HIGHEST = lax.Precision.HIGHEST
NORM_EPS = 1e-06


def carried_in(shard, axis, join, neutral):
    place = lax.axis_index(axis)
    gathered = jax.tree.map(
        lambda a, kind: lax.all_gather(a.astype(kind), axis), shard, (jnp.bfloat16, jnp.bfloat16)
    )
    state = jax.tree.map(lambda a, e: jnp.zeros_like(a) + jnp.asarray(e, a.dtype), shard, neutral)

    def one(lap, state):
        return join(
            state,
            jax.tree.map(
                lambda a, own: lax.dynamic_index_in_dim(a, lap, 0, False).astype(own.dtype),
                gathered,
                shard,
            ),
        )

    return lax.fori_loop(0, place, one, state)


def round_half(tensor):
    return lax.optimization_barrier(tensor.astype(jnp.bfloat16)).astype(jnp.float32)


def forget_attention(query_rows, key_rows, value_rows, forget_rows, fox_gain):
    row_count = query_rows.shape[0]
    head_count = query_rows.shape[1] // HEAD
    kv_count = key_rows.shape[1] // HEAD
    group_size = head_count // kv_count
    score_scale = HEAD ** (-0.5)
    own_first = lax.axis_index("sp") * row_count
    forget_all = lax.all_gather(forget_rows, "sp", axis=0, tiled=True)
    forget_own = forget_rows.reshape(row_count, kv_count, group_size)
    query_heads = query_rows.reshape(row_count, kv_count, group_size, HEAD)
    query_pos = own_first + jnp.arange(row_count, dtype=jnp.int32)
    start_state = (
        jnp.full((row_count, kv_count, group_size), -1e30, jnp.float32),
        jnp.zeros((row_count, kv_count, group_size), jnp.float32),
        jnp.zeros((row_count, kv_count, group_size, HEAD), jnp.float32),
    )
    key_piece = lax.all_gather(key_rows, "sp", axis=0, tiled=True)
    value_piece = lax.all_gather(value_rows, "sp", axis=0, tiled=True)
    piece_rows = key_piece.shape[0]
    block_rows = math.gcd(piece_rows, 512)

    def attend(state):

        def one_block(block_index, inner):
            running_max, totals, weighted = inner
            local_first = (block_index * block_rows).astype(jnp.int32)
            key_block = lax.dynamic_slice_in_dim(key_piece, local_first, block_rows, 0).reshape(
                block_rows, kv_count, HEAD
            )
            value_block = lax.dynamic_slice_in_dim(value_piece, local_first, block_rows, 0).reshape(
                block_rows, kv_count, HEAD
            )
            forget_block = lax.dynamic_slice_in_dim(forget_all, local_first, block_rows, 0).reshape(
                block_rows, kv_count, group_size
            )
            key_pos = local_first + jnp.arange(block_rows, dtype=jnp.int32)
            allowed = (key_pos[None, :] <= query_pos[:, None])[:, None, None, :]
            scores = jnp.einsum(
                "tkgd,skd->tkgs", query_heads, key_block, preferred_element_type=jnp.float32
            )
            scores = (
                scores * score_scale
                + forget_own[..., None]
                - jnp.transpose(forget_block, (1, 2, 0))[None]
            )
            scores = jnp.where(allowed, scores, -1e30)
            new_max = jnp.maximum(running_max, jnp.max(scores, axis=-1))
            rescale = jnp.exp(running_max - new_max)
            weights = jnp.where(allowed, jnp.exp(scores - new_max[..., None]), 0.0)
            totals = totals * rescale + jnp.sum(weights, axis=-1)
            update = jnp.einsum(
                "tkgs,skd->tkgd",
                weights.astype(jnp.bfloat16),
                value_block,
                preferred_element_type=jnp.float32,
            )
            weighted = weighted * rescale[..., None] + update
            return (new_max, totals, weighted)

        return lax.fori_loop(0, piece_rows // block_rows, one_block, state)

    def keep_state(running_state):
        return running_state

    running_max, totals, weighted = lax.cond(
        jnp.int32(0) < own_first + row_count, attend, keep_state, start_state
    )
    attended = (weighted / totals[..., None]).reshape(row_count, head_count, HEAD)
    normed = attended * lax.rsqrt(jnp.mean(attended * attended, axis=-1, keepdims=True) + NORM_EPS)
    return (
        (normed * fox_gain.reshape(head_count, HEAD))
        .reshape(row_count, head_count * HEAD)
        .astype(jnp.bfloat16)
    )


def product(left, right, form):
    return jnp.einsum(form, left, right, precision=HIGHEST)


def delta_attention(recept_rows, key_rows, value_rows, learn_rows, decay_rows, lin_gain):
    row_count = recept_rows.shape[0]
    head_count = recept_rows.shape[1] // HEAD
    span_count = row_count // SPAN

    def arrange(tensor):
        return jnp.transpose(
            tensor.astype(jnp.float32).reshape(span_count, SPAN, head_count, HEAD), (0, 2, 1, 3)
        )

    recept = arrange(recept_rows)
    key_float = arrange(key_rows)
    value_float = arrange(value_rows)
    learn_rate = jax.nn.sigmoid(arrange(learn_rows))
    unit_keys = key_float * lax.rsqrt(
        jnp.sum(key_float * key_float, axis=-1, keepdims=True) + NORM_EPS
    )
    log_decay = -jnp.exp(arrange(decay_rows))
    strict_lower = jnp.tril(jnp.ones((SPAN, SPAN), jnp.float32), -1)
    with_diagonal = jnp.tril(jnp.ones((SPAN, SPAN), jnp.float32))
    identity_head = jnp.broadcast_to(jnp.eye(HEAD, dtype=jnp.float32), (head_count, HEAD, HEAD))
    identity_span = jnp.broadcast_to(jnp.eye(SPAN, dtype=jnp.float32), (head_count, SPAN, SPAN))
    zero_state = jnp.zeros((head_count, HEAD, HEAD), jnp.float32)

    def one_span(state, inputs):
        recept_t, key_t, value_t, unit_t, rate_t, fall_t = inputs
        inclusive = jnp.cumsum(fall_t, axis=1)
        grown = jnp.exp(inclusive)
        shrunk = jnp.exp(-inclusive)
        erase_in = -unit_t * jnp.exp(inclusive - fall_t)
        read_in = recept_t * grown
        erase_out = unit_t * rate_t * shrunk
        write_out = key_t * shrunk
        padded_values = jnp.concatenate([value_t, jnp.zeros_like(value_t)], axis=-1)
        mix_erase = product(erase_in, erase_out, "hid,hjd->hij") * strict_lower
        mix_write = product(erase_in, write_out, "hid,hjd->hij") * strict_lower
        read_erase = product(read_in, erase_out, "hid,hjd->hij") * with_diagonal
        read_write = product(read_in, write_out, "hid,hjd->hij") * with_diagonal
        right_side = product(erase_in, state, "hid,hrd->hir") + product(
            mix_write, padded_values, "hij,hjr->hir"
        )
        erased = jax.scipy.linalg.solve_triangular(
            identity_span - mix_erase, right_side, lower=True, unit_diagonal=True
        )
        outputs = (
            product(read_in, state, "hid,hrd->hir")
            + product(read_erase, erased, "hij,hjr->hir")
            + product(read_write, padded_values, "hij,hjr->hir")
        )
        final_grow = grown[:, -1, :]
        state = (
            state * final_grow[:, None, :]
            + product(erased, erase_out * final_grow[:, None, :], "hlr,hld->hrd")
            + product(padded_values, write_out * final_grow[:, None, :], "hlr,hld->hrd")
        )
        return (state, outputs)

    start_state = jnp.concatenate([zero_state, identity_head], axis=1)
    final_state, outputs = lax.scan(
        one_span, start_state, (recept, key_float, value_float, unit_keys, learn_rate, log_decay)
    )
    local_read = outputs[..., :HEAD]
    carried_read = outputs[..., HEAD:]

    def chain(earlier, later):
        return (
            product(earlier[0], later[0], "hij,hjk->hik"),
            product(earlier[1], later[0], "hij,hjk->hik") + later[1],
        )

    entry_map, entry_state = carried_in(
        (final_state[:, HEAD:], final_state[:, :HEAD]), "sp", chain, (identity_head, zero_state)
    )
    readout = local_read + jnp.einsum(
        "hvk,nhtk->nhtv", entry_state, carried_read, precision=HIGHEST
    )
    readout = jnp.transpose(readout, (0, 2, 1, 3)).reshape(row_count, head_count, HEAD)
    centred = readout - jnp.mean(readout, axis=-1, keepdims=True)
    normed = centred * lax.rsqrt(jnp.mean(centred * centred, axis=-1, keepdims=True) + HEAD * 1e-05)
    return (
        (normed * lin_gain.reshape(head_count, HEAD))
        .reshape(row_count, head_count * HEAD)
        .astype(jnp.bfloat16)
    )


def shards(
    queries,
    keys,
    values,
    forget_cache,
    fox_gain,
    receptance,
    lin_keys,
    lin_values,
    learn_logit,
    decay_log,
    lin_gain,
    out_fox_weight,
    out_lin_weight,
):
    fox_out = forget_attention(queries[0], keys[0], values[0], forget_cache[0], fox_gain)
    lin_out = delta_attention(
        receptance[0], lin_keys[0], lin_values[0], learn_logit[0], decay_log[0], lin_gain
    )
    fox_weight, lin_weight = (
        lax.all_gather(out_fox_weight, "fs", axis=1, tiled=True),
        lax.all_gather(out_lin_weight, "fs", axis=1, tiled=True),
    )
    partial_value = jnp.dot(fox_out, fox_weight, preferred_element_type=jnp.float32)
    partial_value = partial_value + jnp.dot(lin_out, lin_weight, preferred_element_type=jnp.float32)
    summed = lax.psum_scatter(
        round_half(partial_value).astype(jnp.bfloat16), "tp", scatter_dimension=0, tiled=True
    )
    return summed[None]


def solution(mesh):
    return jax.shard_map(
        shards,
        mesh=mesh,
        in_specs=(
            P("fs", "sp", "tp"),
            P("fs", "sp", "tp"),
            P("fs", "sp", "tp"),
            P("fs", "sp", "tp"),
            P("tp"),
            P("fs", "sp", "tp"),
            P("fs", "sp", "tp"),
            P("fs", "sp", "tp"),
            P("fs", "sp", "tp"),
            P("fs", "sp", "tp"),
            P("tp"),
            P("tp", "fs"),
            P("tp", "fs"),
        ),
        out_specs=P("fs", ("sp", "tp"), None),
        check_vma=False,
    )
```

profile of v0, /device:TPU:0, one launch (start us, length us, event | category | flops | bytes accessed | tf_op | source)
XLA Modules:
  0.0 230.0 jit_solution(1138776864522754009)
XLA Ops:
  6.5 0.7 all-gather.8.cloned.1.call-update
  7.3 0.7 all-gather.10.cloned.1.call-update
  8.1 1.2 reshape.164
  10.2 1.1 reshape.163
  11.3 1.0 neg.24
  13.0 106.6 %while.46 = (s32[]{:T(128)}, f32[4,128,64]{1,2,0:T(8,128)S(1)}, f32[4,4,64,128]{3,2,1,0:T(8,128)}, f32[4,4,64,64]{3,1,2,0:T(4,128)}, f32[4,4,64,64]{3,1,2,0:T(4,...) while((s32[]{:T(128)}, f32[4,128,64]{1,2,0:T(8,128)S(1)}, ...), condition=%wide.region_10.11_spmd.clone.clone, body=%wide.region_8.10_spmd.clone.clone.sunk | while | flops 253308992 | bytes 5993869 | solution.py:178
  13.0 0.9 constant_dynamic-slice_fusion.20
  14.1 0.9 constant_dynamic-slice_fusion.19
  15.6 19.7 %custom-call.11 = f32[4,1,64,64]{2,3,1,0:T(8,128)S(1)} custom-call(f32[4,1,64,64]{3,2,1,0:T(8,128)S(1)} %fusion.172), custom_call_target="InvertDiagBlocksLowerTriangular" | custom-call | tf_op jit(solution)/shard_map/while/body/eval_jaxpr/jit(_solve_triangular)/vmap()/triangular_solve | solution.py:161
  35.3 0.4 convolution_multiply_fusion.7
  36.2 0.4 fusion.173
  37.5 0.4 convolution_multiply_fusion.9
  37.9 0.9 fusion.176
  38.8 0.4 convolution_add_fusion.11
  39.2 0.4 convolution_add_fusion.12
  39.6 0.9 constant_dynamic-slice_fusion.20
  40.7 0.9 constant_dynamic-slice_fusion.19
  42.2 19.7 %custom-call.11 = f32[4,1,64,64]{2,3,1,0:T(8,128)S(1)} custom-call(f32[4,1,64,64]{3,2,1,0:T(8,128)S(1)} %fusion.172), custom_call_target="InvertDiagBlocksLowerTriangular" | custom-call | tf_op jit(solution)/shard_map/while/body/eval_jaxpr/jit(_solve_triangular)/vmap()/triangular_solve | solution.py:161
  61.9 0.4 convolution_multiply_fusion.7
  62.9 0.4 fusion.173
  64.2 0.4 convolution_multiply_fusion.9
  64.5 0.9 fusion.176
  65.5 0.4 convolution_add_fusion.11
  65.9 0.4 convolution_add_fusion.12
  66.3 0.9 constant_dynamic-slice_fusion.20
  67.4 0.9 constant_dynamic-slice_fusion.19
  68.9 19.7 %custom-call.11 = f32[4,1,64,64]{2,3,1,0:T(8,128)S(1)} custom-call(f32[4,1,64,64]{3,2,1,0:T(8,128)S(1)} %fusion.172), custom_call_target="InvertDiagBlocksLowerTriangular" | custom-call | tf_op jit(solution)/shard_map/while/body/eval_jaxpr/jit(_solve_triangular)/vmap()/triangular_solve | solution.py:161
  88.6 0.4 convolution_multiply_fusion.7
  89.5 0.4 fusion.173
  91.2 0.9 fusion.176
  92.1 0.4 convolution_add_fusion.11
  92.5 0.4 convolution_add_fusion.12
  92.9 0.9 constant_dynamic-slice_fusion.20
  94.0 0.9 constant_dynamic-slice_fusion.19
  95.5 19.7 %custom-call.11 = f32[4,1,64,64]{2,3,1,0:T(8,128)S(1)} custom-call(f32[4,1,64,64]{3,2,1,0:T(8,128)S(1)} %fusion.172), custom_call_target="InvertDiagBlocksLowerTriangular" | custom-call | tf_op jit(solution)/shard_map/while/body/eval_jaxpr/jit(_solve_triangular)/vmap()/triangular_solve | solution.py:161
  115.2 0.4 convolution_multiply_fusion.7
  116.2 0.4 fusion.173
  117.8 0.9 fusion.176
  118.8 0.4 convolution_add_fusion.11
  119.2 0.4 convolution_add_fusion.12
  119.7 15.7 %all-gather.3 = bf16[16,64,64]{2,1,0:T(8,128)(2,1)S(1)} all-gather(bf16[4,64,64]{2,1,0:T(8,128)(2,1)S(1)} %get-tuple-element.533), channel_id=5, replica_groups=mesh['sp'=4,'fs'=4,'tp'=2] {'sp'}, dimensions={0}, use_global_device_ids=true | all-gather | bytes 163840 | tf_op jit(solution)/shard_map/all_gather | solution.py:19
  135.4 14.6 %all-gather.4 = bf16[16,64,64]{2,1,0:T(8,128)(2,1)S(1)} all-gather(bf16[4,64,64]{2,1,0:T(8,128)(2,1)S(1)} %get-tuple-element.532), channel_id=6, replica_groups=mesh['sp'=4,'fs'=4,'tp'=2] {'sp'}, dimensions={0}, use_global_device_ids=true | all-gather | bytes 163840 | tf_op jit(solution)/shard_map/all_gather | solution.py:19
  150.0 1.0 copy-done
  151.4 1.7 fusion.65
  153.7 0.8 copy.73
  154.9 0.8 copy.72
  156.0 13.2 %all-gather.1 = f32[1,1024,4]{1,2,0:T(4,128)S(1)} all-gather(f32[1,256,4]{1,2,0:T(4,128)S(1)} %copy-done.10), channel_id=3, replica_groups=mesh['sp'=4,'fs'=4,'tp'=2] {'sp'}, dimensions={1}, use_global_device_ids=true | all-gather | bytes 20480 | tf_op jit(solution)/shard_map/all_gather | solution.py:47
  169.2 14.5 %all-gather = bf16[1,1024,128]{1,2,0:T(8,128)(2,1)S(1)} all-gather(bf16[1,256,128]{1,2,0:T(8,128)(2,1)S(1)} %copy.55), channel_id=2, replica_groups=mesh['sp'=4,'fs'=4,'tp'=2] {'sp'}, dimensions={1}, use_global_device_ids=true | all-gather | bytes 327680 | tf_op jit(solution)/shard_map/all_gather | solution.py:56
  183.7 14.0 %all-gather.2 = bf16[1,1024,128]{1,2,0:T(8,128)(2,1)S(1)} all-gather(bf16[1,256,128]{1,2,0:T(8,128)(2,1)S(1)} %copy.56), channel_id=4, replica_groups=mesh['sp'=4,'fs'=4,'tp'=2] {'sp'}, dimensions={1}, use_global_device_ids=true | all-gather | bytes 327680 | tf_op jit(solution)/shard_map/all_gather | solution.py:57
  197.7 10.5 %conditional.1 = (f32[256,2,2]{0,2,1:T(2,128)}, f32[256,2,2,64]{0,3,2,1:T(8,128)}) conditional(s32[]{:T(128)} %convert_element_type.58, () %tuple.38, (s32[]{:T(128)}, s32[256]{0:T(256)S(1)}, bf16[1,256,256]{2,1,0:T(8,128)(2,1)S(1)}, bf16[1024,128]{0,1:T(8,128)(2,1)S(1)}, f32[1,256,4]{1,2,0:T(4,128)S(1)}, /*index=5*/f32[1024,4]{0,1:T(4,128)S(1)}, ...), branch_computations={%region_0.0_spmd, %region_1.6_spmd} | conditional | flops 140318464 | bytes 8662403 | solution.py:104
  197.7 0.8 copy.57
  198.5 9.7 %while.44 = (s32[]{:T(128)}, f32[256,2,2]{0,2,1:T(2,128)S(1)}, f32[256,2,2]{0,2,1:T(2,128)}, f32[256,2,2,64]{0,3,2,1:T(8,128)}, s32[256]{0:T(256)S(1)}, /*index=...) while((s32[]{:T(128)}, f32[256,2,2]{0,2,1:T(2,128)S(1)}, ...), condition=%wide.wide.region_5.5_spmd.clone, body=%wide.wide.region_2.4_spmd.clone.sunk | while | flops 140318208 | bytes 8373459 | solution.py:99
  198.7 1.6 fusion.181
  200.3 0.4 fusion.183
  200.7 0.6 fusion.184
  201.4 1.2 fusion.185
  202.8 1.6 fusion.181
  204.4 0.4 fusion.183
  204.8 1.3 fusion.184
  206.1 2.1 fusion.185
  208.2 1.1 multiply_reduce_fusion.2
  209.5 1.7 fusion.67
  211.2 2.7 %fusion.54 = bf16[256,2048]{1,0:T(8,128)(2,1)} fusion(f32[256,2048]{1,0:T(8,128)S(1)} %fusion.67, bf16[256,2048]{1,0:T(8,128)(2,1)} %all-gather.10.cloned.1.call-done, f32[256,256]{1,0:T(8,128)S(1)} %copy-done.1, f32[256,256]{1,0:T(8,128)S(1)} %reshape.160, f32[256,256]{1,0:T(8,128)S(1)} %copy-done.2, f32[256]{0:T(256)S(1)} %copy-done.13), kind=kOutput, calls=%fused_computation.87 | convolution fusion | flops 269746176 | bytes 4981760 | tf_op jit(solution)/shard_map/dot_general | solution.py:230
  213.9 9.5 %reduce-scatter.2.cloned.1.call-done = bf16[128,2048]{1,0:T(8,128)(2,1)} async-done(((bf16[256,2048]{1,0:T(8,128)(2,1)}), bf16[128,2048]{1,0:T(8,128)(2,1)}) %reduce-scatter.2.cloned.1.call-update) | async-done | bytes 524304 | tf_op jit(solution)/shard_map/reduce_scatter | solution.py:231
  (151 shorter events, 13.2 us)
Async XLA Ops:
  6.5 3.6 %copy-start.4 = (bf16[1,256,256]{2,1,0:T(8,128)(2,1)S(1)}, bf16[1,256,256]{2,1,0:T(8,128)(2,1)}, u32[]{:S(2)}) copy-start(bf16[1,256,256]{2,1,0:T(8,128)(2,1)} %param.29) | copy-start | bytes 393220
  6.5 202.9 %all-gather.8.cloned.1.call-start = ((), (), s32[]{:S(2)}) async-start(), calls=%async_computation.1 | async-start | bytes 1310720 | tf_op jit(solution)/shard_map/all_gather | solution.py:226
  7.3 4.0 %copy-start.3 = (f32[1,256,256]{2,1,0:T(8,128)S(1)}, f32[1,256,256]{2,1,0:T(8,128)}, u32[]{:S(2)}) copy-start(f32[1,256,256]{2,1,0:T(8,128)} %param.30) | copy-start | bytes 786436
  7.3 203.9 %all-gather.10.cloned.1.call-start = ((), (), s32[]{:S(2)}) async-start(), calls=%async_computation.2 | async-start | bytes 1310720 | tf_op jit(solution)/shard_map/all_gather | solution.py:227
  8.0 215.4 %reduce-scatter.2.cloned.1.call-start = ((), (), s32[]{:S(2)}) async-start(), calls=%async_computation.3 | async-start | bytes 1572864 | tf_op jit(solution)/shard_map/reduce_scatter | solution.py:231
  9.6 2.7 %copy-start.5 = (bf16[1,256,256]{2,1,0:T(8,128)(2,1)S(1)}, bf16[1,256,256]{2,1,0:T(8,128)(2,1)}, u32[]{:S(2)}) copy-start(bf16[1,256,256]{2,1,0:T(8,128)(2,1)} %param.28) | copy-start | bytes 393220
  9.7 2.9 %copy-start.6 = (bf16[1,256,256]{2,1,0:T(8,128)(2,1)S(1)}, bf16[1,256,256]{2,1,0:T(8,128)(2,1)}, u32[]{:S(2)}) copy-start(bf16[1,256,256]{2,1,0:T(8,128)(2,1)} %param.26) | copy-start | bytes 393220
  150.0 1.0 copy-start
  153.1 2.7 %copy-start.8 = (bf16[1,256,128]{2,1,0:T(8,128)(2,1)S(1)}, bf16[1,256,128]{2,1,0:T(8,128)(2,1)}, u32[]{:S(2)}) copy-start(bf16[1,256,128]{2,1,0:T(8,128)(2,1)} %param.22) | copy-start | bytes 196612
  153.1 2.8 %copy-start.9 = (bf16[1,256,128]{2,1,0:T(8,128)(2,1)S(1)}, bf16[1,256,128]{2,1,0:T(8,128)(2,1)}, u32[]{:S(2)}) copy-start(bf16[1,256,128]{2,1,0:T(8,128)(2,1)} %param.23) | copy-start | bytes 196612
  153.1 2.9 %copy-start.10 = (f32[1,256,4]{1,2,0:T(4,128)S(1)}, f32[1,256,4]{1,2,0:T(4,128)}, u32[]{:S(2)}) copy-start(f32[1,256,4]{1,2,0:T(4,128)} %param.24) | copy-start | bytes 12292
  153.4 44.3 %copy-start.7 = (bf16[1,256,256]{2,1,0:T(8,128)(2,1)S(1)}, bf16[1,256,256]{2,1,0:T(8,128)(2,1)}, u32[]{:S(2)}) copy-start(bf16[1,256,256]{2,1,0:T(8,128)(2,1)} %param.21) | copy-start | bytes 393220
  197.7 11.6 %copy-start.12 = (f32[256]{0:T(256)S(1)}, f32[256]{0:T(256)}, u32[]{:S(2)}) copy-start(f32[256]{0:T(256)} %param.25) | copy-start | bytes 3076
  197.7 0.8 copy-start.11
  208.2 3.0 %copy-start.1 = (f32[256,256]{1,0:T(8,128)S(1)}, f32[256,256]{1,0:T(8,128)}, u32[]{:S(2)}) copy-start(f32[256,256]{1,0:T(8,128)} %copy.73) | copy-start | bytes 786436
  208.2 3.0 %copy-start.2 = (f32[256,256]{1,0:T(8,128)S(1)}, f32[256,256]{1,0:T(8,128)}, u32[]{:S(2)}) copy-start(f32[256,256]{1,0:T(8,128)} %copy.72) | copy-start | bytes 786436
  208.2 3.0 %copy-start.13 = (f32[256]{0:T(256)S(1)}, f32[256]{0:T(256)}, u32[]{:S(2)}) copy-start(f32[256]{0:T(256)} %param.31) | copy-start | bytes 3076
Sparse Core Ops, SparseCore 0:
  9.2 29.8 all-gather.7
  40.9 27.0 all-gather.9
  214.0 9.3 reduce-scatter.1
where the time goes:
time: 231 us; the launch traced here: 230 us
  other arithmetic  85.3 us (37%)
  blocking collectives  71.9 us (31%)
  matrix products  30.9 us (13%)
  local copies, waits for them, and re-layouts  16.6 us (7%)
  between operations  13.5 us (6%)
  waiting for transfers between devices  11 us (5%)
    another operation x12, other arithmetic, one_span(): jax.scipy.linalg.solve_triangular(identity_span - mix_erase, right_side,...  79 us
    all_gather x2, blocking collectives, carried_in(): lax.all_gather(a.astype(kind), axis)  30.2 us
    dot_general x44, matrix products, product(): return jnp.einsum(form, left, right, precision=HIGHEST)  16.7 us
    all_gather x1, blocking collectives, forget_attention(): key_piece = lax.all_gather(key_rows, 'sp', axis=0, tiled=True)  14.5 us
    all_gather x1, blocking collectives, forget_attention(): value_piece = lax.all_gather(value_rows, 'sp', axis=0, tiled=True)  14 us
    all_gather x1, blocking collectives, forget_attention(): forget_all = lax.all_gather(forget_rows, 'sp', axis=0, tiled=True)  13.2 us
    reduce_scatter x1, waiting for transfers between devices, shards(): lax.psum_scatter(round_half(partial_value).astype(jnp.bfloat16), 'tp', sc...  9.53 us
    dynamic_slice x20, local copies, waits for them, and re-layouts, delta_attention(): lax.scan(one_span, start_state, (recept, key_float, value_float, unit_key...  7.59 us
  transfers between devices with their start and end apart: 3, of which 1 were waited for; matrix products, arithmetic and copies ran while one was open for 56% of the time, Pallas kernels for 0%

commit v1 on v0

v1 whole, which is shorter than its diff:
```python
import functools

import jax
import jax.numpy as jnp
from jax import lax
from jax.experimental import pallas as pl
from jax.experimental.pallas import tpu as pltpu
from jax.sharding import PartitionSpec as P

HEAD = 64
SPAN = 64
SPAN_BITS = SPAN.bit_length() - 1
NORM_EPS = 1e-06
MESH = pl.DeviceIdType.MESH
F32 = jnp.float32
BF16 = jnp.bfloat16


def pieces(x, count):
    out = []
    for _ in range(count - 1):
        top = x.astype(BF16)
        out.append(top)
        x = x - top.astype(F32)
    out.append(x.astype(BF16))
    return out


def dot(a, b, dims, passes):
    run = functools.partial(lax.dot_general, dimension_numbers=dims, preferred_element_type=F32)
    if passes == 1:
        return run(a.astype(BF16), b.astype(BF16))
    a_hi, a_lo = pieces(a, 2)
    if passes == 2:
        return run(a_hi, b.astype(BF16)) + run(a_lo, b.astype(BF16))
    b_hi, b_lo = pieces(b, 2)
    return run(a_hi, b_hi) + (run(a_hi, b_lo) + run(a_lo, b_hi))


NN = (((1,), (0,)), ((), ()))
NT = (((1,), (1,)), ((), ()))
BNN = (((2,), (1,)), ((0,), (0,)))
BNT = (((2,), (2,)), ((0,), (0,)))


def iota(shape, dim):
    return lax.broadcasted_iota(jnp.int32, shape, dim)


def delta_maps(recept, keys, values, learn, decay_log, passes):
    rows, width = recept.shape
    spans, heads = rows // SPAN, width // HEAD
    i, j = iota((rows, rows), 0), iota((rows, rows), 1)
    lower = ((i >> SPAN_BITS) == (j >> SPAN_BITS)) & (j <= i)
    lower = jnp.where(lower, 1.0, 0.0).astype(BF16)
    ones = head_ones(width)
    keys, values, recept = keys.astype(F32), values.astype(F32), recept.astype(F32)
    rate = jax.nn.sigmoid(learn.astype(F32))
    unit = keys * lax.rsqrt(dot(keys * keys, ones, NN, 2) + NORM_EPS)
    fall = -jnp.exp(decay_log)
    inclusive = sum(
        lax.dot_general(lower, part, NN, preferred_element_type=F32) for part in pieces(fall, 3)
    )
    last = jnp.concatenate(
        [
            jnp.broadcast_to(inclusive[(c + 1) * SPAN - 1 : (c + 1) * SPAN], (SPAN, width))
            for c in range(spans)
        ],
        axis=0,
    )
    shrunk = jnp.exp(-inclusive)
    tail = jnp.exp(last - inclusive)
    unit_rate = unit * rate

    def cut(x):
        return jnp.stack(
            [
                x[c * SPAN : (c + 1) * SPAN, h * HEAD : (h + 1) * HEAD]
                for c in range(spans)
                for h in range(heads)
            ]
        )

    def cut_turned(x):
        x = jnp.transpose(x)
        return jnp.stack(
            [
                x[h * HEAD : (h + 1) * HEAD, c * SPAN : (c + 1) * SPAN]
                for c in range(spans)
                for h in range(heads)
            ]
        )

    erase_in = cut(-unit * jnp.exp(inclusive - fall))
    read_in = cut(recept * jnp.exp(inclusive))
    erase_out, write_out = cut(unit_rate * shrunk), cut(keys * shrunk)
    value = cut(values)
    count = spans * heads
    zero = jnp.zeros((count, SPAN, HEAD), F32)

    i, j = iota((2 * SPAN, 2 * SPAN), 0), iota((2 * SPAN, 2 * SPAN), 1)
    allowed = (j & (SPAN - 1)) < (i & (SPAN - 1)) + (i >> SPAN_BITS)
    mixes = dot(
        jnp.concatenate([erase_in, read_in], 1),
        jnp.concatenate([erase_out, write_out], 1),
        BNT,
        passes,
    )
    mixes = jnp.where(allowed[None], mixes, 0.0)
    erase = mixes[:, :SPAN, :SPAN]
    i, j = iota((SPAN, SPAN), 0), iota((SPAN, SPAN), 1)

    def level(bit):
        same = (i >> (bit + 1)) == (j >> (bit + 1))
        return (same & (((i >> bit) & 1) == 1) & (((j >> bit) & 1) == 0))[None]

    inverse = jnp.where((i == j)[None], 1.0, jnp.where(level(0), erase, 0.0))
    for bit in range(1, SPAN_BITS):
        step = jnp.where(level(bit), erase, 0.0)
        inverse = inverse + dot(inverse, dot(step, inverse, BNN, passes), BNN, passes)
    mixed_values = dot(mixes, jnp.concatenate([zero, value], 1), BNN, passes)
    erased = dot(
        inverse, jnp.concatenate([erase_in, mixed_values[:, :SPAN]], 2), BNN, passes
    )
    outs = jnp.concatenate([read_in, mixed_values[:, SPAN:]], 2) + dot(
        mixes[:, SPAN:, :SPAN], erased, BNN, passes
    )
    turned = jnp.concatenate([cut_turned(unit_rate * tail), cut_turned(keys * tail)], 2)
    grow = jnp.exp(last)
    grow = jnp.concatenate([cut(grow), zero], 2)
    i, j = iota((HEAD, 2 * HEAD), 0), iota((HEAD, 2 * HEAD), 1)
    maps = dot(
        turned,
        jnp.concatenate([erased, jnp.concatenate([zero, value], 2)], 1),
        BNN,
        passes,
    ) + jnp.where((i == j)[None], grow, 0.0)
    right = (j >= HEAD)[None]
    before = maps[:heads]
    carried = [outs[:heads]]
    for c in range(1, spans):
        here = slice(c * heads, (c + 1) * heads)
        carried.append(
            dot(outs[here][:, :, :HEAD], before, BNN, passes) + jnp.where(right, outs[here], 0.0)
        )
        before = dot(maps[here][:, :, :HEAD], before, BNN, passes) + jnp.where(
            right, maps[here], 0.0
        )
    return jnp.concatenate(carried, 0), before


def head_ones(width):
    bits = HEAD.bit_length() - 1
    i, j = iota((width, width), 0), iota((width, width), 1)
    return jnp.where((i >> bits) == (j >> bits), 1.0, 0.0).astype(BF16)


def kernel(
    sizes, passes,
    q_ref, k_ref, v_ref, f_ref, fox_gain_ref,
    r_ref, lk_ref, lv_ref, learn_ref, decay_ref, lin_gain_ref,
    wf_ref, wl_ref,
    out_ref,
    k_buf, v_buf, f_buf, map_own, map_buf, w_buf, carried_ref,
    max_ref, total_ref, acc_ref, act_ref, part_own, part_buf,
    k_send, v_send, f_send, k_recv, v_recv, f_recv,
    map_send, map_recv, w_send, w_recv, part_send, part_recv, local_sem,
):
    n_sp, n_fs, n_tp = sizes
    me, fs, tp = lax.axis_index("sp"), lax.axis_index("fs"), lax.axis_index("tp")
    rows, width = q_ref.shape
    heads = width // HEAD
    kv_heads = k_ref.shape[1] // HEAD
    group = heads // kv_heads
    lin_heads = r_ref.shape[1] // HEAD
    spans = rows // SPAN
    lin_width = r_ref.shape[1]
    block = wf_ref.shape[1]
    half = rows // n_tp

    barrier = pltpu.get_barrier_semaphore()

    def greet(step, _):
        pl.semaphore_signal(
            barrier, inc=1, device_id={"sp": lax.rem(me + step, n_sp)}, device_id_type=MESH
        )
        return 0

    lax.fori_loop(1, n_sp, greet, 0)
    for step in range(1, n_fs):
        pl.semaphore_signal(
            barrier, inc=1, device_id={"fs": lax.rem(fs + step, n_fs)}, device_id_type=MESH
        )
    for step in range(1, n_tp):
        pl.semaphore_signal(
            barrier, inc=1, device_id={"tp": lax.rem(tp + step, n_tp)}, device_id_type=MESH
        )
    pl.semaphore_wait(barrier, n_sp + n_fs + n_tp - 3)

    def to_later(src, buf, send, recv, other):
        return pltpu.make_async_remote_copy(
            src_ref=src, dst_ref=buf.at[me], send_sem=send.at[other], recv_sem=recv.at[me],
            device_id={"sp": other}, device_id_type=MESH,
        )

    def from_earlier(src, buf, send, recv, other):
        return pltpu.make_async_remote_copy(
            src_ref=src, dst_ref=buf.at[other], send_sem=send.at[other], recv_sem=recv.at[other],
            device_id={"sp": other}, device_id_type=MESH,
        )

    shared = (
        (k_ref, k_buf, k_send, k_recv),
        (v_ref, v_buf, v_send, v_recv),
        (f_ref, f_buf, f_send, f_recv),
    )

    def send_block(other, _):
        for item in shared:
            to_later(*item, other).start()
        return 0

    lax.fori_loop(me + 1, n_sp, send_block, 0)

    def weight_copy(which, step):
        src = (wf_ref, wl_ref)[which]
        return pltpu.make_async_remote_copy(
            src_ref=src, dst_ref=w_buf.at[fs, which],
            send_sem=w_send.at[which, step], recv_sem=w_recv.at[which, fs],
            device_id={"fs": lax.rem(fs + step, n_fs)}, device_id_type=MESH,
        )

    def weight_wait(which, source):
        return pltpu.make_async_remote_copy(
            src_ref=(wf_ref, wl_ref)[which], dst_ref=w_buf.at[source, which],
            send_sem=w_send.at[which, 0], recv_sem=w_recv.at[which, source],
            device_id={"fs": source}, device_id_type=MESH,
        )

    for which in range(2):
        for step in range(1, n_fs):
            weight_copy(which, step).start()
    own = [
        pltpu.make_async_copy((wf_ref, wl_ref)[which], w_buf.at[fs, which], local_sem.at[which])
        for which in range(2)
    ]
    for copy in own:
        copy.start()

    carried, maps = delta_maps(
        r_ref[...], lk_ref[...], lv_ref[...], learn_ref[...], decay_ref[...], passes
    )
    map_own[...] = maps.astype(BF16)
    carried_ref[...] = carried

    def send_map(other, _):
        to_later(map_own, map_buf, map_send, map_recv, other).start()
        return 0

    lax.fori_loop(me + 1, n_sp, send_map, 0)

    scaled = (q_ref[...].astype(F32) * HEAD ** (-0.5)).astype(BF16)

    def attend(key_block, value_block, forget_block, first):
        forget = jnp.transpose(forget_block)
        turned = jnp.transpose(value_block)
        if first:
            seen = iota((rows, rows), 0) <= iota((rows, rows), 1)
        for h in range(heads):
            kv = slice(h // group * HEAD, (h // group + 1) * HEAD)
            scores = lax.dot_general(
                key_block[:, kv], scaled[:, h * HEAD : (h + 1) * HEAD], NT,
                preferred_element_type=F32,
            ) - forget[:, h : h + 1]
            if first:
                scores = jnp.where(seen, scores, -1e30)
            top = jnp.max(scores, axis=0, keepdims=True)
            if not first:
                old = max_ref[h]
                top = jnp.maximum(old, top)
                rescale = jnp.exp(old - top)
            weights = jnp.exp(scores - top)
            total = jnp.sum(weights, axis=0, keepdims=True)
            update = lax.dot_general(
                turned[kv], weights.astype(BF16), NN, preferred_element_type=F32
            )
            if not first:
                total = total + total_ref[h] * rescale
                update = update + acc_ref[h] * rescale
            max_ref[h] = top
            total_ref[h] = total
            acc_ref[h] = update

    attend(k_ref[...], v_ref[...], f_ref[...], True)

    def earlier(step, _):
        other = me - 1 - step
        for item in shared:
            from_earlier(*item, other).wait_recv()
        attend(k_buf[other], v_buf[other], f_buf[other], False)
        return 0

    lax.fori_loop(0, me, earlier, 0)
    normed = []
    for h in range(heads):
        attended = acc_ref[h] / total_ref[h]
        normed.append(
            attended
            * lax.rsqrt(jnp.mean(attended * attended, axis=0, keepdims=True) + NORM_EPS)
        )
    fox_out = jnp.transpose(jnp.concatenate(normed, axis=0)) * fox_gain_ref[...]
    act_ref[:, :width] = fox_out.astype(BF16)

    def join(other, state):
        from_earlier(map_own, map_buf, map_send, map_recv, other).wait_recv()
        step = map_buf[other]
        return dot(step[:, :, :HEAD].astype(F32), state, BNN, passes) + step[:, :, HEAD:].astype(F32)

    state = lax.fori_loop(0, me, join, jnp.zeros((lin_heads, HEAD, HEAD), F32))
    eye = jnp.where(iota((HEAD, HEAD), 0) == iota((HEAD, HEAD), 1), 1.0, 0.0)
    eye = jnp.broadcast_to(eye[None], (lin_heads, HEAD, HEAD))
    state = jnp.concatenate([state, eye], axis=1)
    read = []
    for c in range(spans):
        here = dot(carried_ref[c * lin_heads : (c + 1) * lin_heads], state, BNN, 3)
        read.append(jnp.concatenate([here[h] for h in range(lin_heads)], axis=1))
    read = jnp.concatenate(read, axis=0)
    ones = head_ones(lin_width)
    centred = read - dot(read, ones, NN, 2) * (1.0 / HEAD)
    spread = dot(centred * centred, ones, NN, 2) * (1.0 / HEAD)
    lin_out = centred * lax.rsqrt(spread + HEAD * 1e-05) * lin_gain_ref[...]
    act_ref[:, width:] = lin_out.astype(BF16)

    def project(first, source):
        act = act_ref[pl.ds(pl.multiple_of(first, half), half), :]
        return lax.dot_general(
            act[:, :width], w_buf[source, 0], NN, preferred_element_type=F32
        ) + lax.dot_general(act[:, width:], w_buf[source, 1], NN, preferred_element_type=F32)

    def part_copy(step, source):
        return pltpu.make_async_remote_copy(
            src_ref=part_own.at[step - 1, source], dst_ref=part_buf.at[step - 1, source],
            send_sem=part_send.at[step - 1, source], recv_sem=part_recv.at[step - 1, source],
            device_id={"tp": lax.rem(tp + step, n_tp)}, device_id_type=MESH,
        )

    for copy in own:
        copy.wait()
    for hop in range(n_fs):
        source = lax.rem(fs + hop, n_fs)
        if hop > 0:
            for which in range(2):
                weight_wait(which, source).wait_recv()
        for step in range(1, n_tp):
            part_own[step - 1, source] = project(
                lax.rem(tp + step, n_tp) * half, source
            ).astype(BF16)
            part_copy(step, source).start()
    for source in range(n_fs):
        total = project(tp * half, source).astype(BF16).astype(F32)
        for step in range(1, n_tp):
            part_copy(step, source).wait_recv()
            total = total + part_buf[step - 1, source].astype(F32)
        out_ref[:, source * block : (source + 1) * block] = total.astype(BF16)

    def drain(other, _):
        for item in shared + ((map_own, map_buf, map_send, map_recv),):
            to_later(*item, other).wait_send()
        return 0

    lax.fori_loop(me + 1, n_sp, drain, 0)
    for which in range(2):
        for step in range(1, n_fs):
            weight_copy(which, step).wait_send()
    for source in range(n_fs):
        for step in range(1, n_tp):
            part_copy(step, source).wait_send()


def shards(
    sizes, passes,
    queries, keys, values, forget_cache, fox_gain, receptance, lin_keys, lin_values,
    learn_logit, decay_log, lin_gain, out_fox_weight, out_lin_weight,
):
    n_sp, n_fs, n_tp = sizes
    _, rows, width = queries.shape
    kv_width = keys.shape[2]
    lin_width = receptance.shape[2]
    heads, lin_heads = width // HEAD, lin_width // HEAD
    fox_rows, block = out_fox_weight.shape
    half = rows // n_tp
    forget = jnp.transpose(forget_cache[0])
    forget = jnp.pad(forget, ((0, -forget.shape[0] % 8), (0, 0)))
    dma = pltpu.SemaphoreType.DMA
    vmem = pltpu.VMEM
    out = pl.pallas_call(
        functools.partial(kernel, sizes, passes),
        out_shape=jax.ShapeDtypeStruct((half, n_fs * block), BF16),
        in_specs=[pl.BlockSpec(memory_space=vmem)] * 13,
        out_specs=pl.BlockSpec(memory_space=vmem),
        scratch_shapes=[
            vmem((n_sp, rows, kv_width), BF16),
            vmem((n_sp, rows, kv_width), BF16),
            vmem((n_sp,) + forget.shape, F32),
            vmem((lin_heads, HEAD, 2 * HEAD), BF16),
            vmem((n_sp, lin_heads, HEAD, 2 * HEAD), BF16),
            vmem((n_fs, 2, fox_rows, block), BF16),
            vmem((rows // SPAN * lin_heads, SPAN, 2 * HEAD), F32),
            vmem((heads, 1, rows), F32),
            vmem((heads, 1, rows), F32),
            vmem((heads, HEAD, rows), F32),
            vmem((rows, width + lin_width), BF16),
            vmem((n_tp - 1, n_fs, half, block), BF16),
            vmem((n_tp - 1, n_fs, half, block), BF16),
        ]
        + [dma((n_sp,))] * 8
        + [dma((2, n_fs))] * 2
        + [dma((n_tp - 1, n_fs))] * 2
        + [dma((2,))],
        compiler_params=pltpu.CompilerParams(
            collective_id=0, has_side_effects=True, vmem_limit_bytes=60 * 1024 * 1024
        ),
    )(
        queries[0], keys[0], values[0], forget, fox_gain[None],
        receptance[0], lin_keys[0], lin_values[0], learn_logit[0], decay_log[0], lin_gain[None],
        out_fox_weight, out_lin_weight,
    )
    return out[None]


def solution(mesh, passes=3):
    sizes = tuple(mesh.shape[name] for name in ("sp", "fs", "tp"))
    rows = P("fs", "sp", "tp")
    return jax.shard_map(
        functools.partial(shards, sizes, passes),
        mesh=mesh,
        in_specs=(rows,) * 4 + (P("tp"),) + (rows,) * 5 + (P("tp"), P("tp", "fs"), P("tp", "fs")),
        out_specs=P("fs", ("sp", "tp"), None),
        check_vma=False,
    )
```

time: 231 us -> 37.4 us (0.16)
  other arithmetic: 85.3 us -> 0 us
  blocking collectives: 71.9 us -> 0 us
  Pallas kernels: 0 us -> 34 us
  matrix products: 30.9 us -> 0 us
  between operations: 13.5 us -> 0.01 us
  local copies, waits for them, and re-layouts: 16.6 us -> 3.17 us
  waiting for transfers between devices: 11 us -> 0 us
    another operation x16 -> x0, other arithmetic: 79.5 us -> none  [the longest x12 79 us: one_span(): jax.scipy.linalg.solve_triangular(identity_span - mix_erase, right_side,...]
    all_gather x5 -> x0, blocking collectives: 71.9 us -> none  [the longest x2 30.2 us: carried_in(): lax.all_gather(a.astype(kind), axis)]
    pallas_call x0 -> x1, Pallas kernels: none -> 34 us  [shards(): pl.pallas_call(functools.partial(kernel, sizes, passes), out_shape=jax.Sh...]
    dot_general x51 -> x0, matrix products: 29.3 us -> none  [the longest x44 16.7 us: product(): return jnp.einsum(form, left, right, precision=HIGHEST)]
    reduce_scatter x1 -> x0, waiting for transfers between devices: 9.53 us -> none  [shards(): lax.psum_scatter(round_half(partial_value).astype(jnp.bfloat16), 'tp', sc...]
    dynamic_slice x24 -> x0, local copies, waits for them, and re-layouts: 7.65 us -> none  [the longest x20 7.59 us: delta_attention(): lax.scan(one_span, start_state, (recept, key_float, value_float, unit_key...]
  transfers between devices with their start and end apart: 3 -> 0, of which waited for: 1 -> 0; matrix products, arithmetic and copies ran while one was open for 56% -> 0% of each run, Pallas kernels for 0% -> 0%
where the time goes in v1:
time: 37.4 us; the launch traced here: 37.2 us
  Pallas kernels  34 us (91%)
  local copies, waits for them, and re-layouts  3.17 us (8%)
    pallas_call x1, Pallas kernels, shards(): pl.pallas_call(functools.partial(kernel, sizes, passes), out_shape=jax.Sh...  34 us
    unnamed x3, local copies, waits for them, and re-layouts  2.57 us

profile of v1, /device:TPU:0, one launch (start us, length us, event | category | flops | bytes accessed | tf_op | source)
XLA Modules:
  0.0 37.2 jit_solution(719405576448878501)
XLA Ops:
  0.0 0.0 copy-start
  0.0 0.7 %copy-done = f32[1,256,4]{1,2,0:T(4,128)S(1)} copy-done((f32[1,256,4]{1,2,0:T(4,128)S(1)}, f32[1,256,4]{1,2,0:T(4,128)}, u32[]{:S(2)}) %copy-start) | copy-done | bytes 4120
  0.7 0.6 %pad.4.f_ref = f32[8,256]{1,0:T(8,128)} pad(f32[4,256]{1,0:T(4,128)S(1)} %bitcast.23, f32[]{:T(128)} %constant.2.clone.1), padding=0_4x0_0 | pad | bytes 12292 | tf_op jit(solution)/shard_map/jit(_pad)/pad | solution.py:393
  1.3 34.0 %shard_map.127 = bf16[128,2048]{1,0:T(8,128)(2,1)} custom-call(bf16[256,256]{1,0:T(8,128)(2,1)} %bitcast.16, bf16[256,128]{1,0:T(8,128)(2,1)} %bitcast.21, bf16[256,128]{1,0:T(8,128)(2,1)} %bitcast.22, f32[8,256]{1,0:T(8,128)} %pad.4.f_ref, f32[1,256]{1,0:T(1,128)} %bitcast.24, bf16[256,256]{1,0:T(8,128)(2,1)} %bitcast.17, bf16[256,256]{1,0:T(8,128)(2,1)} %bitcast.18, ...), custom_call_target="tpu_custom_call" | custom-call | tf_op jit(solution)/shard_map/pallas_call | solution.py:396
  35.3 1.9 %copy.15 = bf16[1,128,2048]{2,1,0:T(8,128)(2,1)} copy(bf16[1,128,2048]{2,1,0:T(8,128)(2,1)} %bitcast.14) | data formatting | bytes 1048576
Async XLA Ops:
  0.0 0.7 %copy-start = (f32[1,256,4]{1,2,0:T(4,128)S(1)}, f32[1,256,4]{1,2,0:T(4,128)}, u32[]{:S(2)}) copy-start(f32[1,256,4]{1,2,0:T(4,128)} %param.16) | copy-start | bytes 12292

commit v2 on v1

--- a/solution.py
+++ b/solution.py
@@ -157,10 +157,11 @@
 
 def kernel(
     sizes, passes,
-    q_ref, k_ref, v_ref, f_ref, fox_gain_ref,
-    r_ref, lk_ref, lv_ref, learn_ref, decay_ref, lin_gain_ref,
-    wf_ref, wl_ref,
+    q_in, k_in, v_in, f_in, fox_gain_ref,
+    r_in, lk_in, lv_in, learn_in, decay_in, lin_gain_ref,
+    wf_in, wl_in,
     out_ref,
+    q_ref, r_ref, lk_ref, lv_ref, learn_ref, decay_ref,
     k_buf, v_buf, f_buf, map_own, map_buf, w_buf, carried_ref,
     max_ref, total_ref, acc_ref, act_ref, part_own, part_buf,
     k_send, v_send, f_send, k_recv, v_recv, f_recv,
@@ -170,13 +171,25 @@
     me, fs, tp = lax.axis_index("sp"), lax.axis_index("fs"), lax.axis_index("tp")
     rows, width = q_ref.shape
     heads = width // HEAD
-    kv_heads = k_ref.shape[1] // HEAD
+    kv_heads = k_in.shape[1] // HEAD
     group = heads // kv_heads
     lin_heads = r_ref.shape[1] // HEAD
     spans = rows // SPAN
     lin_width = r_ref.shape[1]
-    block = wf_ref.shape[1]
+    block = wf_in.shape[1]
     half = rows // n_tp
+
+    targets = (
+        (k_in, k_buf.at[me]), (v_in, v_buf.at[me]), (f_in, f_buf.at[me]),
+        (wf_in, w_buf.at[fs, 0]), (wl_in, w_buf.at[fs, 1]),
+        (decay_in, decay_ref), (lk_in, lk_ref), (learn_in, learn_ref),
+        (r_in, r_ref), (lv_in, lv_ref), (q_in, q_ref),
+    )
+    loads = [
+        pltpu.make_async_copy(src, dst, local_sem.at[at]) for at, (src, dst) in enumerate(targets)
+    ]
+    for load in loads:
+        load.start()
 
     barrier = pltpu.get_barrier_semaphore()
 
@@ -197,55 +210,67 @@
         )
     pl.semaphore_wait(barrier, n_sp + n_fs + n_tp - 3)
 
-    def to_later(src, buf, send, recv, other):
+    def map_copy(source, other):
         return pltpu.make_async_remote_copy(
-            src_ref=src, dst_ref=buf.at[me], send_sem=send.at[other], recv_sem=recv.at[me],
+            src_ref=map_own, dst_ref=map_buf.at[source],
+            send_sem=map_send.at[other], recv_sem=map_recv.at[source],
             device_id={"sp": other}, device_id_type=MESH,
         )
 
-    def from_earlier(src, buf, send, recv, other):
+    def block_copy(item, source, hop):
+        buf, send, recv = item
         return pltpu.make_async_remote_copy(
-            src_ref=src, dst_ref=buf.at[other], send_sem=send.at[other], recv_sem=recv.at[other],
-            device_id={"sp": other}, device_id_type=MESH,
-        )
-
-    shared = (
-        (k_ref, k_buf, k_send, k_recv),
-        (v_ref, v_buf, v_send, v_recv),
-        (f_ref, f_buf, f_send, f_recv),
-    )
-
-    def send_block(other, _):
-        for item in shared:
-            to_later(*item, other).start()
-        return 0
-
-    lax.fori_loop(me + 1, n_sp, send_block, 0)
-
-    def weight_copy(which, step):
-        src = (wf_ref, wl_ref)[which]
+            src_ref=buf.at[source], dst_ref=buf.at[source],
+            send_sem=send.at[source, hop - 1], recv_sem=recv.at[source],
+            device_id={"sp": lax.rem(me + hop, n_sp)}, device_id_type=MESH,
+        )
+
+    shared = ((k_buf, k_send, k_recv), (v_buf, v_send, v_recv), (f_buf, f_send, f_recv))
+
+    def on_block(source, act):
+        for hop in (1, 2):
+            if hop < n_sp:
+
+                @pl.when(me + hop < n_sp)
+                def _():
+                    for item in shared:
+                        act(block_copy(item, source, hop))
+
+    for load in loads[:3]:
+        load.wait()
+    on_block(me, lambda copy: copy.start())
+
+    def weight_copy(which, source, step, target):
         return pltpu.make_async_remote_copy(
-            src_ref=src, dst_ref=w_buf.at[fs, which],
-            send_sem=w_send.at[which, step], recv_sem=w_recv.at[which, fs],
-            device_id={"fs": lax.rem(fs + step, n_fs)}, device_id_type=MESH,
-        )
-
-    def weight_wait(which, source):
-        return pltpu.make_async_remote_copy(
-            src_ref=(wf_ref, wl_ref)[which], dst_ref=w_buf.at[source, which],
-            send_sem=w_send.at[which, 0], recv_sem=w_recv.at[which, source],
-            device_id={"fs": source}, device_id_type=MESH,
-        )
-
-    for which in range(2):
-        for step in range(1, n_fs):
-            weight_copy(which, step).start()
-    own = [
-        pltpu.make_async_copy((wf_ref, wl_ref)[which], w_buf.at[fs, which], local_sem.at[which])
-        for which in range(2)
-    ]
-    for copy in own:
+            src_ref=w_buf.at[source, which], dst_ref=w_buf.at[source, which],
+            send_sem=w_send.at[which, step], recv_sem=w_recv.at[which, source],
+            device_id={"fs": target}, device_id_type=MESH,
+        )
+
+    relayed = n_fs == 4
+    if relayed:
+        beside = fs + 1 - 2 * lax.rem(fs, 2)
+        across = lax.rem(fs + 2, 4)
+        direct = [
+            weight_copy(0, fs, 0, beside), weight_copy(1, fs, 0, across),
+            weight_copy(1, fs, 1, beside), weight_copy(0, fs, 1, across),
+        ]
+        passed = [weight_copy(0, beside, 2, across), weight_copy(1, across, 2, beside)]
+        order = [fs, beside, across, lax.rem(beside + 2, 4)]
+    else:
+        direct = [
+            weight_copy(which, fs, step - 1, lax.rem(fs + step, n_fs))
+            for which in range(2)
+            for step in range(1, n_fs)
+        ]
+        passed = []
+        order = [lax.rem(fs + step, n_fs) for step in range(n_fs)]
+    for load in loads[3:5]:
+        load.wait()
+    for copy in direct:
         copy.start()
+    for load in loads[5:]:
+        load.wait()
 
     carried, maps = delta_maps(
         r_ref[...], lk_ref[...], lv_ref[...], learn_ref[...], decay_ref[...], passes
@@ -254,15 +279,20 @@
     carried_ref[...] = carried
 
     def send_map(other, _):
-        to_later(map_own, map_buf, map_send, map_recv, other).start()
+        map_copy(me, other).start()
         return 0
 
     lax.fori_loop(me + 1, n_sp, send_map, 0)
 
+    for copy in passed:
+        copy.wait_recv()
+        copy.start()
+
     scaled = (q_ref[...].astype(F32) * HEAD ** (-0.5)).astype(BF16)
 
     def attend(key_block, value_block, forget_block, first):
-        forget = jnp.transpose(forget_block)
+        pad = jnp.zeros((-heads % 8, rows), F32)
+        forget = jnp.transpose(jnp.concatenate([forget_block, pad], axis=0))
         turned = jnp.transpose(value_block)
         if first:
             seen = iota((rows, rows), 0) <= iota((rows, rows), 1)
@@ -291,12 +321,25 @@
             total_ref[h] = total
             acc_ref[h] = update
 
-    attend(k_ref[...], v_ref[...], f_ref[...], True)
+    attend(k_buf[me], v_buf[me], f_buf[me], True)
+
+    def pass_on(step, _):
+        source = me - 2 * step
+        for item in shared:
+            block_copy(item, source, 1).wait_recv()
+        on_block(source, lambda copy: copy.start())
+        return 0
+
+    lax.fori_loop(1, me // 2 + 1, pass_on, 0)
 
     def earlier(step, _):
         other = me - 1 - step
-        for item in shared:
-            from_earlier(*item, other).wait_recv()
+
+        @pl.when(lax.rem(step, 2) == 0)
+        def _():
+            for item in shared:
+                block_copy(item, other, 1).wait_recv()
+
         attend(k_buf[other], v_buf[other], f_buf[other], False)
         return 0
 
@@ -312,7 +355,7 @@
     act_ref[:, :width] = fox_out.astype(BF16)
 
     def join(other, state):
-        from_earlier(map_own, map_buf, map_send, map_recv, other).wait_recv()
+        map_copy(other, other).wait_recv()
         step = map_buf[other]
         return dot(step[:, :, :HEAD].astype(F32), state, BNN, passes) + step[:, :, HEAD:].astype(F32)
 
@@ -344,13 +387,10 @@
             device_id={"tp": lax.rem(tp + step, n_tp)}, device_id_type=MESH,
         )
 
-    for copy in own:
-        copy.wait()
-    for hop in range(n_fs):
-        source = lax.rem(fs + hop, n_fs)
-        if hop > 0:
-            for which in range(2):
-                weight_wait(which, source).wait_recv()
+    for hop, source in enumerate(order):
+        for which in range(2):
+            if hop > 0 and not (relayed and which == hop - 1):
+                weight_copy(which, source, 0, source).wait_recv()
         for step in range(1, n_tp):
             part_own[step - 1, source] = project(
                 lax.rem(tp + step, n_tp) * half, source
@@ -361,17 +401,21 @@
         for step in range(1, n_tp):
             part_copy(step, source).wait_recv()
             total = total + part_buf[step - 1, source].astype(F32)
-        out_ref[:, source * block : (source + 1) * block] = total.astype(BF16)
+        out_ref[:, source * block : (source + 1) * block] = total
 
     def drain(other, _):
-        for item in shared + ((map_own, map_buf, map_send, map_recv),):
-            to_later(*item, other).wait_send()
+        map_copy(me, other).wait_send()
         return 0
 
     lax.fori_loop(me + 1, n_sp, drain, 0)
-    for which in range(2):
-        for step in range(1, n_fs):
-            weight_copy(which, step).wait_send()
+
+    def drain_blocks(step, _):
+        on_block(me - 2 * step, lambda copy: copy.wait_send())
+        return 0
+
+    lax.fori_loop(0, me // 2 + 1, drain_blocks, 0)
+    for copy in direct + passed:
+        copy.wait_send()
     for source in range(n_fs):
         for step in range(1, n_tp):
             part_copy(step, source).wait_send()
@@ -390,15 +434,19 @@
     fox_rows, block = out_fox_weight.shape
     half = rows // n_tp
     forget = jnp.transpose(forget_cache[0])
-    forget = jnp.pad(forget, ((0, -forget.shape[0] % 8), (0, 0)))
     dma = pltpu.SemaphoreType.DMA
     vmem = pltpu.VMEM
+    near = pl.BlockSpec(memory_space=vmem)
+    anywhere = pl.BlockSpec(memory_space=pl.ANY)
     out = pl.pallas_call(
         functools.partial(kernel, sizes, passes),
-        out_shape=jax.ShapeDtypeStruct((half, n_fs * block), BF16),
-        in_specs=[pl.BlockSpec(memory_space=vmem)] * 13,
+        out_shape=jax.ShapeDtypeStruct((half, n_fs * block), F32),
+        in_specs=[anywhere] * 4 + [near] + [anywhere] * 5 + [near] + [anywhere] * 2,
         out_specs=pl.BlockSpec(memory_space=vmem),
-        scratch_shapes=[
+        scratch_shapes=[vmem((rows, width), BF16)]
+        + [vmem((rows, lin_width), BF16)] * 4
+        + [vmem((rows, lin_width), F32)]
+        + [
             vmem((n_sp, rows, kv_width), BF16),
             vmem((n_sp, rows, kv_width), BF16),
             vmem((n_sp,) + forget.shape, F32),
@@ -413,10 +461,11 @@
             vmem((n_tp - 1, n_fs, half, block), BF16),
             vmem((n_tp - 1, n_fs, half, block), BF16),
         ]
-        + [dma((n_sp,))] * 8
+        + [dma((n_sp, 2))] * 3
+        + [dma((n_sp,))] * 5
         + [dma((2, n_fs))] * 2
         + [dma((n_tp - 1, n_fs))] * 2
-        + [dma((2,))],
+        + [dma((11,))],
         compiler_params=pltpu.CompilerParams(
             collective_id=0, has_side_effects=True, vmem_limit_bytes=60 * 1024 * 1024
         ),
@@ -425,7 +474,7 @@
         receptance[0], lin_keys[0], lin_values[0], learn_logit[0], decay_log[0], lin_gain[None],
         out_fox_weight, out_lin_weight,
     )
-    return out[None]
+    return out.astype(BF16)[None]
 
 
 def solution(mesh, passes=3):

time: 37.4 us -> 30.1 us (0.80)
  Pallas kernels: 34 us -> 27.6 us
  local copies, waits for them, and re-layouts: 3.17 us -> 0 us
  other arithmetic: 0 us -> 2.09 us
    pallas_call x1, Pallas kernels: 34 us -> 27.6 us  [shards(): pl.pallas_call(functools.partial(kernel, sizes, passes), out_shape=jax.Sh...]
    unnamed x3 -> x0, local copies, waits for them, and re-layouts: 2.57 us -> none
    broadcast_in_dim x0 -> x1, other arithmetic: none -> 2.09 us  [shards(): return out.astype(BF16)[None]]
    pad x1 -> x0, local copies, waits for them, and re-layouts: 0.6 us -> none  [shards(): forget = jnp.pad(forget, ((0, -forget.shape[0] % 8), (0, 0)))]
where the time goes in v2:
time: 30.1 us; the launch traced here: 29.7 us
  Pallas kernels  27.6 us (92%)
  other arithmetic  2.09 us (7%)
    pallas_call x1, Pallas kernels, shards(): pl.pallas_call(functools.partial(kernel, sizes, passes), out_shape=jax.Sh...  27.6 us
    broadcast_in_dim x1, other arithmetic, shards(): return out.astype(BF16)[None]  2.09 us

profile of v2, /device:TPU:0, one launch (start us, length us, event | category | flops | bytes accessed | tf_op | source)
XLA Modules:
  0.0 29.7 jit_solution(6102639793468175335)
XLA Ops:
  0.0 27.6 %shard_map.127 = f32[128,2048]{1,0:T(8,128)} custom-call(bf16[256,256]{1,0:T(8,128)(2,1)} %bitcast.16, bf16[256,128]{1,0:T(8,128)(2,1)} %bitcast.21, bf16[256,128]{1,0:T(8,128)(2,1)} %bitcast.22, f32[4,256]{1,0:T(4,128)} %bitcast.23, f32[1,256]{1,0:T(1,128)} %bitcast.24, bf16[256,256]{1,0:T(8,128)(2,1)} %bitcast.17, bf16[256,256]{1,0:T(8,128)(2,1)} %bitcast.18, ...), custom_call_target="tpu_custom_call" | custom-call | tf_op jit(solution)/shard_map/pallas_call | solution.py:441
  27.6 2.1 %convert_bitcast_fusion = bf16[1,128,2048]{2,1,0:T(8,128)(2,1)} fusion(f32[128,2048]{1,0:T(8,128)} %shard_map.127), kind=kLoop, calls=%fused_computation | loop fusion | flops 262144 | bytes 1572864 | tf_op jit(solution)/shard_map/broadcast_in_dim | solution.py:477
